TPU v7x, 512 devices: a whole 4x8x8 slice. The times are simulated.
512 devices in a mesh: ep: 32 (over z, x), tp: 16 (over y, core).
Axes of the slice: x: 4, y: 8, z: 8, core: 2. Of those that a mesh axis runs over, the one named last changes fastest.
Arguments:
- queries: bfloat16 [12288, 2048], P('ep', 'tp'), may hold values from -8 to 8
- keys: bfloat16 [12288, 2048], P('ep', 'tp'), may hold values from -8 to 8
- values: bfloat16 [12288, 2048], P('ep', 'tp'), may hold values from -6 to 6
- key_offset: bfloat16 [12288, 16], P('ep', 'tp'), may hold values from -15.25 to -0.4
- rows: bfloat16 [4096, 2048], P('ep'), may hold values from -6 to 6
- gain: float32 [2048], replicated, may hold values from 0.1 to 1.9
- gate_w: bfloat16 [32, 2048, 3584], P('ep', None, 'tp'), may hold values from -0.125 to 0.125
- up_w: bfloat16 [32, 2048, 3584], P('ep', None, 'tp'), may hold values from -0.125 to 0.125
- down_w: bfloat16 [32, 3584, 2048], P('ep', 'tp'), may hold values from -0.09375 to 0.09375
- expert_ids: int32 [4096, 2], P('ep'), may hold values from 0 to 31, all different within a row; in each aligned block of 128 rows (0 to 127, 128 to 255, ...) at most 16 rows name the same one
- route_weights: float32 [4096, 2], P('ep'), may hold values from 0.2 to 1
Outputs:
- attended: bfloat16 [12288, 2048], P('ep', 'tp')
- mixed: bfloat16 [4096, 2048], P('ep')
Inputs may be any that keep to these rules, and one draw needn't show every extreme that they name: `expert_ids`: each token names 2 different experts; among the 128 tokens of one ep index no expert is chosen more than 16 times, and in some such block an expert is chosen exactly 16 times.
All inputs are finite; a program needn't handle non-finite values.
Results may differ from a plain program's by a relative error of at most 0.019.
Values may be sent and summed in bfloat16 or wider, within the bound.
No kernel may reach another device: no remote copies, remote signals or barrier semaphores. Data moves between devices by JAX's collectives and lax.ppermute only.
A program may use at most 128 MiB of HBM per device.

v0:
```python
import jax
import jax.numpy as jnp
from jax import lax
from jax.sharding import PartitionSpec as P

EPSILON = 1e-06


def in_blocks(x, dim, peers):
    before, after = (x.shape[:dim], x.shape[dim + 1 :])
    return jnp.moveaxis(x.reshape(*before, peers, -1, *after), dim, 0)


def sent_and_summed(x, axis, dim):
    parts = in_blocks(x, dim, lax.axis_size(axis))
    arrived = lax.all_to_all(parts, axis, split_axis=0, concat_axis=0, tiled=True)
    return arrived.astype(jnp.float32).sum(axis=0)


def joined_along(parts, dim):
    shape = list(parts.shape[1:])
    shape[dim] *= parts.shape[0]
    return jnp.moveaxis(parts, 0, dim).reshape(shape)


def sent_to_all(x, axis):
    copies = jnp.broadcast_to(x, (lax.axis_size(axis), *x.shape))
    return lax.all_to_all(copies, axis, split_axis=0, concat_axis=0, tiled=True)


def collect(x, axis, dim):
    return joined_along(sent_to_all(x, axis), dim)


def stick_mixer(queries, keys, values, key_offset):
    position = lax.axis_index("ep")
    query_len = queries.shape[0]
    heads = key_offset.shape[1]
    head_dim = queries.shape[1] // heads
    scale = head_dim ** (-0.5)
    query_heads = queries.reshape(query_len, heads, head_dim)
    query_pos = position * query_len + jnp.arange(query_len, dtype=jnp.int32)
    last_row = (position + 1) * query_len
    key_piece = lax.all_gather(keys, "ep", axis=0, tiled=True)
    value_piece = lax.all_gather(values, "ep", axis=0, tiled=True)
    offset_piece = lax.all_gather(key_offset, "ep", axis=0, tiled=True)
    block_count = key_piece.shape[0] // query_len
    key_split = key_piece.reshape(block_count, query_len, heads, head_dim)
    value_split = value_piece.reshape(block_count, query_len, heads, head_dim)
    offset_split = offset_piece.reshape(block_count, query_len, heads)

    def compute_block(key_here, value_here, offset_here, key_start):
        key_pos = key_start + jnp.arange(query_len, dtype=jnp.int32)
        logits = (
            jnp.einsum("qhd,khd->hqk", query_heads, key_here, preferred_element_type=jnp.float32)
            * scale
        )
        logits = logits + offset_here.astype(jnp.float32).T[:, None, :]
        strict = key_pos[None, None, :] < query_pos[None, :, None]
        breaks = jnp.where(strict, jax.nn.log_sigmoid(-logits), 0.0)
        within = lax.cumsum(breaks, axis=2, reverse=True) - breaks
        local = jnp.where(strict, jnp.exp(jax.nn.log_sigmoid(logits) + within), 0.0).astype(
            jnp.bfloat16
        )
        summed = jnp.einsum("hqk,khd->hqd", local, value_here, preferred_element_type=jnp.float32)
        return (summed, jnp.sum(breaks, axis=2))

    def skip_block(key_here, value_here, offset_here, key_start):
        return (
            jnp.zeros((heads, query_len, head_dim), jnp.float32),
            jnp.zeros((heads, query_len), jnp.float32),
        )

    def one_block(args):
        key_here, value_here, offset_here, block_index = args
        key_start = block_index * query_len
        return lax.cond(
            key_start < last_row,
            compute_block,
            skip_block,
            key_here,
            value_here,
            offset_here,
            key_start,
        )

    sums, totals = lax.map(
        one_block, (key_split, value_split, offset_split, jnp.arange(block_count, dtype=jnp.int32))
    )
    sums, totals = (sums, totals)
    later = lax.cumsum(totals, axis=0, reverse=True) - totals
    combined = jnp.einsum("bhq,bhqd->qhd", jnp.exp(later), sums)
    return combined.reshape(query_len, heads * head_dim).astype(jnp.bfloat16)


def routed_experts(rows, gain, gate_w, up_w, down_w, expert_ids, route_weights):
    ep_count = lax.axis_size("ep")
    local_experts = gate_w.shape[0]
    experts_all = ep_count * local_experts
    token_count = rows.shape[0]
    choose_count = expert_ids.shape[1]
    width = rows.shape[1]
    capacity = 2 * choose_count * token_count // experts_all
    rows_float = rows.astype(jnp.float32)
    normed = rows_float * lax.rsqrt(
        jnp.mean(rows_float * rows_float, axis=1, keepdims=True) + EPSILON
    )
    normed = (normed * gain[None, :]).astype(jnp.bfloat16)
    flat_ids = expert_ids.reshape(-1)
    onehot = (flat_ids[:, None] == jnp.arange(experts_all, dtype=jnp.int32)[None, :]).astype(
        jnp.int32
    )
    ranked = jnp.sum((jnp.cumsum(onehot, axis=0) - onehot) * onehot, axis=1)
    token_of = jnp.arange(token_count * choose_count, dtype=jnp.int32) // choose_count
    source_rows = (
        jnp.zeros((experts_all * capacity,), jnp.int32)
        .at[flat_ids * capacity + ranked]
        .set(token_of)
    )
    outgoing = normed[source_rows].reshape(ep_count, local_experts, capacity, width)
    arrived = lax.all_to_all(outgoing, "ep", split_axis=0, concat_axis=0, tiled=True)
    gate_val = jnp.einsum("sxcd,xdf->csxf", arrived, gate_w, preferred_element_type=jnp.float32)
    up_val = jnp.einsum("sxcd,xdf->csxf", arrived, up_w, preferred_element_type=jnp.float32)
    hidden = (jax.nn.silu(gate_val) * up_val).astype(jnp.bfloat16)
    share = sent_and_summed(
        jnp.einsum("csxf,xfd->csxd", hidden, down_w, preferred_element_type=jnp.float32).astype(
            jnp.bfloat16
        ),
        "tp",
        0,
    ).astype(jnp.bfloat16)
    returned = lax.all_to_all(share, "ep", split_axis=1, concat_axis=1, tiled=True)
    whole_slots = collect(returned, "tp", 0)
    flat_out = whole_slots.reshape(capacity * experts_all, width)
    slot_index = ranked * experts_all + flat_ids
    picked = flat_out[slot_index].astype(jnp.float32).reshape(token_count, choose_count, width)
    return jnp.sum(picked * route_weights[:, :, None], axis=1).astype(jnp.bfloat16)


def body(
    queries, keys, values, key_offset, rows, gain, gate_w, up_w, down_w, expert_ids, route_weights
):
    attended = stick_mixer(queries, keys, values, key_offset)
    mixed = routed_experts(rows, gain, gate_w, up_w, down_w, expert_ids, route_weights)
    return (attended, mixed)


def solution(mesh):
    in_specs = (
        P("ep", "tp"),
        P("ep", "tp"),
        P("ep", "tp"),
        P("ep", "tp"),
        P("ep", None),
        P(),
        P("ep", None, "tp"),
        P("ep", None, "tp"),
        P("ep", "tp", None),
        P("ep", None),
        P("ep", None),
    )
    out_specs = (P("ep", "tp"), P("ep", None))
    return jax.shard_map(body, mesh=mesh, in_specs=in_specs, out_specs=out_specs, check_vma=False)
```

profile of v0, /device:TPU:463, one launch (start us, length us, event | category | flops | bytes accessed | tf_op | source)
XLA Modules:
  0.0 519.0 jit_solution(13295193791613204802)
XLA Ops:
  24.6 48.0 %all-to-all-done = bf16[32,1,16,2048]{3,2,1,0:T(8,128)(2,1)S(1)} async-done(((bf16[32,1,16,2048]{3,2,1,0:T(8,128)(2,1)}), bf16[32,1,16,2048]{3,2,1,0:T(8,128)(2,1)S(1)}, u32[]{:S(2)}, u32[]{:S(2)}) %all-to-all-start) | async-done | bytes 2097184 | tf_op jit(solution)/shard_map/all_to_all | solution.py:121
  76.1 58.9 %all_to_all.23 = bf16[16,1,32,1,2048]{4,2,3,1,0:T(8,128)(2,1)S(1)} all-to-all(bf16[16,1,32,1,2048]{4,2,3,1,0:T(8,128)(2,1)S(1)} %fusion.22), channel_id=1, replica_groups=mesh['ep'=32,'tp'=16] {'tp'}, dimensions={0} | all-to-all | bytes 4194304 | tf_op jit(solution)/shard_map/all_to_all | solution.py:16
  138.3 9.8 %all-to-all-start.2 = ((bf16[32,2,1024]{2,1,0:T(2,128)(2,1)}), bf16[32,2,1024]{2,1,0:T(2,128)(2,1)S(1)}, u32[]{:S(2)}, u32[]{:S(2)}) async-start(bf16[32,2,1024]{2,1,0:T(2,128)(2,1)} %reshape.303), calls=%async_computation.2 | async-start | bytes 262144 | tf_op jit(solution)/shard_map/all_to_all | solution.py:132
  148.2 37.1 %all_gather.10 = bf16[12288,1]{0,1:T(2,128)(2,1)S(1)} all-gather(bf16[384,1]{0,1:T(2,128)(2,1)S(1)} %copy-done.1), channel_id=1, replica_groups=mesh['ep'=32,'tp'=16] {'ep'}, dimensions={0}, use_global_device_ids=true | all-gather | bytes 25344 | tf_op jit(solution)/shard_map/all_gather | solution.py:46
  187.4 16.1 %all-to-all-start.3 = ((bf16[16,1,32,1,2048]{4,2,3,1,0:T(8,128)(2,1)}), bf16[16,1,32,1,2048]{4,2,3,1,0:T(8,128)(2,1)}, u32[]{:S(2)}, u32[]{:S(2)}) async-start(bf16[16,1,32,1,2048]{4,2,3,1,0:T(8,128)(2,1)} %broadcast_in_dim.46), calls=%async_computation.3 | async-start | bytes 4194304 | tf_op jit(solution)/shard_map/all_to_all | solution.py:28
  203.7 291.9 %while.13 = (s32[]{:T(128)}, bf16[32,1,384,128]{3,2,1,0:T(8,128)(2,1)}, f32[32,1,384]{2,1,0:T(1,128)S(1)}, s32[32]{0:T(128)S(1)}, s32[]{:T(128)}, /*index=5*/bf1...) while((s32[]{:T(128)}, ...), condition=%wide.region_6.7_spmd.clone, body=%wide.region_0.6_spmd.clone.sunk | while | flops 99241728 | bytes 5957639 | solution.py:87
  204.9 7.2 %conditional.3 = (bf16[1,1,384,128]{3,2,1,0:T(8,128)(2,1)S(1)}, f32[1,1,384]{2,1,0:T(1,128)S(1)}) conditional(s32[]{:T(128)} %convert_element_type.99, () %tuple.52, (s32[]{:T(128)}, s32[]{:T(128)}, bf16[32,384,1,128]{3,1,2,0:T(8,128)(2,1)}, s32[]{:T(128)}, bf16[384,1,128]{2,0,1:T(8,128)(2,1)S(1)}, /*index=5*/bf16[32,384,1]{1,0,2:T(8,128)(2,1)S(1)}, ...), branch_computations={%region_1.1_spmd, %region_2.5_spmd} | conditional | flops 99241728 | bytes 5755680 | solution.py:77
  241.4 7.2 %conditional.3 = (bf16[1,1,384,128]{3,2,1,0:T(8,128)(2,1)S(1)}, f32[1,1,384]{2,1,0:T(1,128)S(1)}) conditional(s32[]{:T(128)} %convert_element_type.99, () %tuple.52, (s32[]{:T(128)}, s32[]{:T(128)}, bf16[32,384,1,128]{3,1,2,0:T(8,128)(2,1)}, s32[]{:T(128)}, bf16[384,1,128]{2,0,1:T(8,128)(2,1)S(1)}, /*index=5*/bf16[32,384,1]{1,0,2:T(8,128)(2,1)S(1)}, ...), branch_computations={%region_1.1_spmd, %region_2.5_spmd} | conditional | flops 99241728 | bytes 5755680 | solution.py:77
  268.8 7.2 %conditional.3 = (bf16[1,1,384,128]{3,2,1,0:T(8,128)(2,1)S(1)}, f32[1,1,384]{2,1,0:T(1,128)S(1)}) conditional(s32[]{:T(128)} %convert_element_type.99, () %tuple.52, (s32[]{:T(128)}, s32[]{:T(128)}, bf16[32,384,1,128]{3,1,2,0:T(8,128)(2,1)}, s32[]{:T(128)}, bf16[384,1,128]{2,0,1:T(8,128)(2,1)S(1)}, /*index=5*/bf16[32,384,1]{1,0,2:T(8,128)(2,1)S(1)}, ...), branch_computations={%region_1.1_spmd, %region_2.5_spmd} | conditional | flops 99241728 | bytes 5755680 | solution.py:77
  277.9 7.2 %conditional.3 = (bf16[1,1,384,128]{3,2,1,0:T(8,128)(2,1)S(1)}, f32[1,1,384]{2,1,0:T(1,128)S(1)}) conditional(s32[]{:T(128)} %convert_element_type.99, () %tuple.52, (s32[]{:T(128)}, s32[]{:T(128)}, bf16[32,384,1,128]{3,1,2,0:T(8,128)(2,1)}, s32[]{:T(128)}, bf16[384,1,128]{2,0,1:T(8,128)(2,1)S(1)}, /*index=5*/bf16[32,384,1]{1,0,2:T(8,128)(2,1)S(1)}, ...), branch_computations={%region_1.1_spmd, %region_2.5_spmd} | conditional | flops 99241728 | bytes 5755680 | solution.py:77
  287.0 7.2 %conditional.3 = (bf16[1,1,384,128]{3,2,1,0:T(8,128)(2,1)S(1)}, f32[1,1,384]{2,1,0:T(1,128)S(1)}) conditional(s32[]{:T(128)} %convert_element_type.99, () %tuple.52, (s32[]{:T(128)}, s32[]{:T(128)}, bf16[32,384,1,128]{3,1,2,0:T(8,128)(2,1)}, s32[]{:T(128)}, bf16[384,1,128]{2,0,1:T(8,128)(2,1)S(1)}, /*index=5*/bf16[32,384,1]{1,0,2:T(8,128)(2,1)S(1)}, ...), branch_computations={%region_1.1_spmd, %region_2.5_spmd} | conditional | flops 99241728 | bytes 5755680 | solution.py:77
  296.1 7.2 %conditional.3 = (bf16[1,1,384,128]{3,2,1,0:T(8,128)(2,1)S(1)}, f32[1,1,384]{2,1,0:T(1,128)S(1)}) conditional(s32[]{:T(128)} %convert_element_type.99, () %tuple.52, (s32[]{:T(128)}, s32[]{:T(128)}, bf16[32,384,1,128]{3,1,2,0:T(8,128)(2,1)}, s32[]{:T(128)}, bf16[384,1,128]{2,0,1:T(8,128)(2,1)S(1)}, /*index=5*/bf16[32,384,1]{1,0,2:T(8,128)(2,1)S(1)}, ...), branch_computations={%region_1.1_spmd, %region_2.5_spmd} | conditional | flops 99241728 | bytes 5755680 | solution.py:77
  305.3 7.2 %conditional.3 = (bf16[1,1,384,128]{3,2,1,0:T(8,128)(2,1)S(1)}, f32[1,1,384]{2,1,0:T(1,128)S(1)}) conditional(s32[]{:T(128)} %convert_element_type.99, () %tuple.52, (s32[]{:T(128)}, s32[]{:T(128)}, bf16[32,384,1,128]{3,1,2,0:T(8,128)(2,1)}, s32[]{:T(128)}, bf16[384,1,128]{2,0,1:T(8,128)(2,1)S(1)}, /*index=5*/bf16[32,384,1]{1,0,2:T(8,128)(2,1)S(1)}, ...), branch_computations={%region_1.1_spmd, %region_2.5_spmd} | conditional | flops 99241728 | bytes 5755680 | solution.py:77
  332.6 7.2 %conditional.3 = (bf16[1,1,384,128]{3,2,1,0:T(8,128)(2,1)S(1)}, f32[1,1,384]{2,1,0:T(1,128)S(1)}) conditional(s32[]{:T(128)} %convert_element_type.99, () %tuple.52, (s32[]{:T(128)}, s32[]{:T(128)}, bf16[32,384,1,128]{3,1,2,0:T(8,128)(2,1)}, s32[]{:T(128)}, bf16[384,1,128]{2,0,1:T(8,128)(2,1)S(1)}, /*index=5*/bf16[32,384,1]{1,0,2:T(8,128)(2,1)S(1)}, ...), branch_computations={%region_1.1_spmd, %region_2.5_spmd} | conditional | flops 99241728 | bytes 5755680 | solution.py:77
  350.9 7.2 %conditional.3 = (bf16[1,1,384,128]{3,2,1,0:T(8,128)(2,1)S(1)}, f32[1,1,384]{2,1,0:T(1,128)S(1)}) conditional(s32[]{:T(128)} %convert_element_type.99, () %tuple.52, (s32[]{:T(128)}, s32[]{:T(128)}, bf16[32,384,1,128]{3,1,2,0:T(8,128)(2,1)}, s32[]{:T(128)}, bf16[384,1,128]{2,0,1:T(8,128)(2,1)S(1)}, /*index=5*/bf16[32,384,1]{1,0,2:T(8,128)(2,1)S(1)}, ...), branch_computations={%region_1.1_spmd, %region_2.5_spmd} | conditional | flops 99241728 | bytes 5755680 | solution.py:77
  396.5 7.2 %conditional.3 = (bf16[1,1,384,128]{3,2,1,0:T(8,128)(2,1)S(1)}, f32[1,1,384]{2,1,0:T(1,128)S(1)}) conditional(s32[]{:T(128)} %convert_element_type.99, () %tuple.52, (s32[]{:T(128)}, s32[]{:T(128)}, bf16[32,384,1,128]{3,1,2,0:T(8,128)(2,1)}, s32[]{:T(128)}, bf16[384,1,128]{2,0,1:T(8,128)(2,1)S(1)}, /*index=5*/bf16[32,384,1]{1,0,2:T(8,128)(2,1)S(1)}, ...), branch_computations={%region_1.1_spmd, %region_2.5_spmd} | conditional | flops 99241728 | bytes 5755680 | solution.py:77
  405.6 7.2 %conditional.3 = (bf16[1,1,384,128]{3,2,1,0:T(8,128)(2,1)S(1)}, f32[1,1,384]{2,1,0:T(1,128)S(1)}) conditional(s32[]{:T(128)} %convert_element_type.99, () %tuple.52, (s32[]{:T(128)}, s32[]{:T(128)}, bf16[32,384,1,128]{3,1,2,0:T(8,128)(2,1)}, s32[]{:T(128)}, bf16[384,1,128]{2,0,1:T(8,128)(2,1)S(1)}, /*index=5*/bf16[32,384,1]{1,0,2:T(8,128)(2,1)S(1)}, ...), branch_computations={%region_1.1_spmd, %region_2.5_spmd} | conditional | flops 99241728 | bytes 5755680 | solution.py:77
  414.8 7.2 %conditional.3 = (bf16[1,1,384,128]{3,2,1,0:T(8,128)(2,1)S(1)}, f32[1,1,384]{2,1,0:T(1,128)S(1)}) conditional(s32[]{:T(128)} %convert_element_type.99, () %tuple.52, (s32[]{:T(128)}, s32[]{:T(128)}, bf16[32,384,1,128]{3,1,2,0:T(8,128)(2,1)}, s32[]{:T(128)}, bf16[384,1,128]{2,0,1:T(8,128)(2,1)S(1)}, /*index=5*/bf16[32,384,1]{1,0,2:T(8,128)(2,1)S(1)}, ...), branch_computations={%region_1.1_spmd, %region_2.5_spmd} | conditional | flops 99241728 | bytes 5755680 | solution.py:77
  433.0 7.2 %conditional.3 = (bf16[1,1,384,128]{3,2,1,0:T(8,128)(2,1)S(1)}, f32[1,1,384]{2,1,0:T(1,128)S(1)}) conditional(s32[]{:T(128)} %convert_element_type.99, () %tuple.52, (s32[]{:T(128)}, s32[]{:T(128)}, bf16[32,384,1,128]{3,1,2,0:T(8,128)(2,1)}, s32[]{:T(128)}, bf16[384,1,128]{2,0,1:T(8,128)(2,1)S(1)}, /*index=5*/bf16[32,384,1]{1,0,2:T(8,128)(2,1)S(1)}, ...), branch_computations={%region_1.1_spmd, %region_2.5_spmd} | conditional | flops 99241728 | bytes 5755680 | solution.py:77
  451.2 7.2 %conditional.3 = (bf16[1,1,384,128]{3,2,1,0:T(8,128)(2,1)S(1)}, f32[1,1,384]{2,1,0:T(1,128)S(1)}) conditional(s32[]{:T(128)} %convert_element_type.99, () %tuple.52, (s32[]{:T(128)}, s32[]{:T(128)}, bf16[32,384,1,128]{3,1,2,0:T(8,128)(2,1)}, s32[]{:T(128)}, bf16[384,1,128]{2,0,1:T(8,128)(2,1)S(1)}, /*index=5*/bf16[32,384,1]{1,0,2:T(8,128)(2,1)S(1)}, ...), branch_computations={%region_1.1_spmd, %region_2.5_spmd} | conditional | flops 99241728 | bytes 5755680 | solution.py:77
  460.4 7.2 %conditional.3 = (bf16[1,1,384,128]{3,2,1,0:T(8,128)(2,1)S(1)}, f32[1,1,384]{2,1,0:T(1,128)S(1)}) conditional(s32[]{:T(128)} %convert_element_type.99, () %tuple.52, (s32[]{:T(128)}, s32[]{:T(128)}, bf16[32,384,1,128]{3,1,2,0:T(8,128)(2,1)}, s32[]{:T(128)}, bf16[384,1,128]{2,0,1:T(8,128)(2,1)S(1)}, /*index=5*/bf16[32,384,1]{1,0,2:T(8,128)(2,1)S(1)}, ...), branch_computations={%region_1.1_spmd, %region_2.5_spmd} | conditional | flops 99241728 | bytes 5755680 | solution.py:77
  469.5 7.2 %conditional.3 = (bf16[1,1,384,128]{3,2,1,0:T(8,128)(2,1)S(1)}, f32[1,1,384]{2,1,0:T(1,128)S(1)}) conditional(s32[]{:T(128)} %convert_element_type.99, () %tuple.52, (s32[]{:T(128)}, s32[]{:T(128)}, bf16[32,384,1,128]{3,1,2,0:T(8,128)(2,1)}, s32[]{:T(128)}, bf16[384,1,128]{2,0,1:T(8,128)(2,1)S(1)}, /*index=5*/bf16[32,384,1]{1,0,2:T(8,128)(2,1)S(1)}, ...), branch_computations={%region_1.1_spmd, %region_2.5_spmd} | conditional | flops 99241728 | bytes 5755680 | solution.py:77
  478.6 7.2 %conditional.3 = (bf16[1,1,384,128]{3,2,1,0:T(8,128)(2,1)S(1)}, f32[1,1,384]{2,1,0:T(1,128)S(1)}) conditional(s32[]{:T(128)} %convert_element_type.99, () %tuple.52, (s32[]{:T(128)}, s32[]{:T(128)}, bf16[32,384,1,128]{3,1,2,0:T(8,128)(2,1)}, s32[]{:T(128)}, bf16[384,1,128]{2,0,1:T(8,128)(2,1)S(1)}, /*index=5*/bf16[32,384,1]{1,0,2:T(8,128)(2,1)S(1)}, ...), branch_computations={%region_1.1_spmd, %region_2.5_spmd} | conditional | flops 99241728 | bytes 5755680 | solution.py:77
  487.7 7.2 %conditional.3 = (bf16[1,1,384,128]{3,2,1,0:T(8,128)(2,1)S(1)}, f32[1,1,384]{2,1,0:T(1,128)S(1)}) conditional(s32[]{:T(128)} %convert_element_type.99, () %tuple.52, (s32[]{:T(128)}, s32[]{:T(128)}, bf16[32,384,1,128]{3,1,2,0:T(8,128)(2,1)}, s32[]{:T(128)}, bf16[384,1,128]{2,0,1:T(8,128)(2,1)S(1)}, /*index=5*/bf16[32,384,1]{1,0,2:T(8,128)(2,1)S(1)}, ...), branch_computations={%region_1.1_spmd, %region_2.5_spmd} | conditional | flops 99241728 | bytes 5755680 | solution.py:77
  (557 shorter events, 412.2 us)
Async XLA Ops:
  7.2 68.2 %copy-start = (bf16[1,224,2048]{2,1,0:T(8,128)(2,1)S(1)}, bf16[1,224,2048]{2,1,0:T(8,128)(2,1)}, u32[]{:S(2)}) copy-start(bf16[1,224,2048]{2,1,0:T(8,128)(2,1)} %param.23) | copy-start | bytes 2752516
  7.2 196.4 %all-gather.3.cloned.1.call-start = ((), (), s32[]{:S(2)}) async-start(), calls=%async_computation.4 | async-start | bytes 3244032 | tf_op jit(solution)/shard_map/all_gather | solution.py:44
  17.3 55.3 %all-to-all-start = ((bf16[32,1,16,2048]{3,2,1,0:T(8,128)(2,1)}), bf16[32,1,16,2048]{3,2,1,0:T(8,128)(2,1)S(1)}, u32[]{:S(2)}, u32[]{:S(2)}) async-start(bf16[32,1,16,2048]{3,2,1,0:T(8,128)(2,1)} %bitcast.23), calls=%async_computation | async-start | bytes 4194304 | tf_op jit(solution)/shard_map/all_to_all | solution.py:121
  23.9 179.8 %all-gather.5.cloned.1.call-start = ((), (), s32[]{:S(2)}) async-start(), calls=%async_computation.5 | async-start | bytes 3244032 | tf_op jit(solution)/shard_map/all_gather | solution.py:45
  72.6 2.0 copy-start.3
  135.1 13.1 %copy-start.1 = (bf16[384,1]{0,1:T(2,128)(2,1)S(1)}, bf16[384,1]{0,1:T(2,128)(2,1)}, u32[]{:S(2)}) copy-start(bf16[384,1]{0,1:T(2,128)(2,1)} %param.18) | copy-start | bytes 2308
  135.1 50.4 %copy-start.2 = (f32[128,2]{0,1:T(2,128)S(1)}, f32[128,2]{0,1:T(2,128)}, u32[]{:S(2)}) copy-start(f32[128,2]{0,1:T(2,128)} %param.25) | copy-start | bytes 3076
  138.3 47.3 %all-to-all-start.2 = ((bf16[32,2,1024]{2,1,0:T(2,128)(2,1)}), bf16[32,2,1024]{2,1,0:T(2,128)(2,1)S(1)}, u32[]{:S(2)}, u32[]{:S(2)}) async-start(bf16[32,2,1024]{2,1,0:T(2,128)(2,1)} %reshape.303), calls=%async_computation.2 | async-start | bytes 262144 | tf_op jit(solution)/shard_map/all_to_all | solution.py:132
  187.4 16.2 %copy-start.4 = (bf16[384,128]{1,0:T(8,128)(2,1)S(1)}, bf16[384,128]{1,0:T(8,128)(2,1)}, u32[]{:S(2)}) copy-start(bf16[384,128]{1,0:T(8,128)(2,1)} %param.15) | copy-start | bytes 294916
  187.4 313.0 %all-to-all-start.3 = ((bf16[16,1,32,1,2048]{4,2,3,1,0:T(8,128)(2,1)}), bf16[16,1,32,1,2048]{4,2,3,1,0:T(8,128)(2,1)}, u32[]{:S(2)}, u32[]{:S(2)}) async-start(bf16[16,1,32,1,2048]{4,2,3,1,0:T(8,128)(2,1)} %broadcast_in_dim.46), calls=%async_computation.3 | async-start | bytes 4194304 | tf_op jit(solution)/shard_map/all_to_all | solution.py:28
Sparse Core Ops, SparseCore 0:
  11.1 85.3 all-gather.2
  99.7 81.6 all-gather.4
where the time goes:
time: 522 us; the launch traced here: 519 us
  other arithmetic  151 us (29%)
  blocking collectives  96.1 us (18%)
  matrix products  92.5 us (18%)
  local copies, waits for them, and re-layouts  59.5 us (11%)
  waiting for transfers between devices  49.4 us (9%)
  starting transfers between devices  32.6 us (6%)
  loops' own time  23.3 us (4%)
  between operations  14.3 us (3%)
    another operation x66, other arithmetic  113 us
    all_to_all x1, blocking collectives, sent_and_summed(): lax.all_to_all(parts, axis, split_axis=0, concat_axis=0, tiled=True)  58.9 us
    all_to_all x1, waiting for transfers between devices, routed_experts(): lax.all_to_all(outgoing, 'ep', split_axis=0, concat_axis=0, tiled=True)  48 us
    dot_general x32, matrix products, compute_block(): jnp.einsum('qhd,khd->hqk', query_heads, key_here, preferred_element_type=...  47.9 us
    dot_general x32, matrix products, compute_block(): jnp.einsum('hqk,khd->hqd', local, value_here, preferred_element_type=jnp....  37.3 us
    all_gather x1, blocking collectives, stick_mixer(): offset_piece = lax.all_gather(key_offset, 'ep', axis=0, tiled=True)  37.1 us
    convert_element_type x32, other arithmetic, compute_block(): jnp.where(strict, jnp.exp(jax.nn.log_sigmoid(logits) + within), 0.0)  27.7 us
    another operation x1, loops' own time, stick_mixer(): lax.map(one_block, (key_split, value_split, offset_split, jnp.arange(bloc...  21.2 us
  transfers between devices with their start and end apart: 5, of which 1 were waited for; matrix products, arithmetic and copies ran while one was open for 56% of the time, Pallas kernels for 0%

commit v1 on v0

--- a/solution.py
+++ b/solution.py
@@ -43,7 +43,10 @@
     last_row = (position + 1) * query_len
     key_piece = lax.all_gather(keys, "ep", axis=0, tiled=True)
     value_piece = lax.all_gather(values, "ep", axis=0, tiled=True)
-    offset_piece = lax.all_gather(key_offset, "ep", axis=0, tiled=True)
+    size = lax.axis_size("ep")
+    shards = jnp.stack([key_offset for _ in range(size)])
+    shards = lax.all_to_all(shards, "ep", split_axis=0, concat_axis=0)
+    offset_piece = jnp.concatenate(shards, axis=0)
     block_count = key_piece.shape[0] // query_len
     key_split = key_piece.reshape(block_count, query_len, heads, head_dim)
     value_split = value_piece.reshape(block_count, query_len, heads, head_dim)

time: 522 us -> 505 us (0.967)
  the two profiles are of different devices: /device:TPU:463 before, /device:TPU:486 now
where the time goes in v1:
time: 505 us; the launch traced here: 502 us
  other arithmetic  152 us (30%)
  waiting for transfers between devices  118 us (23%)
  matrix products  93.9 us (19%)
  local copies, waits for them, and re-layouts  60.4 us (12%)
  starting transfers between devices  40.1 us (8%)
  loops' own time  23.3 us (5%)
  between operations  14.3 us (3%)
    another operation x66, other arithmetic  113 us
    all_to_all x1, waiting for transfers between devices, routed_experts(): lax.all_to_all(outgoing, 'ep', split_axis=0, concat_axis=0, tiled=True)  50.5 us
    dot_general x32, matrix products, compute_block(): jnp.einsum('qhd,khd->hqk', query_heads, key_here, preferred_element_type=...  47.9 us
    all_to_all x1, waiting for transfers between devices, sent_and_summed(): lax.all_to_all(parts, axis, split_axis=0, concat_axis=0, tiled=True)  44.6 us
    dot_general x32, matrix products, compute_block(): jnp.einsum('hqk,khd->hqd', local, value_here, preferred_element_type=jnp....  37.3 us
    convert_element_type x32, other arithmetic, compute_block(): jnp.where(strict, jnp.exp(jax.nn.log_sigmoid(logits) + within), 0.0)  27.7 us
    another operation x1, loops' own time, stick_mixer(): lax.map(one_block, (key_split, value_split, offset_split, jnp.arange(bloc...  21.2 us
    dynamic_update_slice x64, local copies, waits for them, and re-layouts, stick_mixer(): lax.map(one_block, (key_split, value_split, offset_split, jnp.arange(bloc...  21 us
  transfers between devices with their start and end apart: 7, of which 5 were waited for; matrix products, arithmetic and copies ran while one was open for 59% of the time, Pallas kernels for 0%

profile of v1, /device:TPU:486, one launch (start us, length us, event | category | flops | bytes accessed | tf_op | source)
XLA Modules:
  0.0 501.8 jit_solution(5852398344939566793)
XLA Ops:
  25.2 50.5 %all-to-all-done.1 = bf16[32,1,16,2048]{3,2,1,0:T(8,128)(2,1)S(1)} async-done(((bf16[32,1,16,2048]{3,2,1,0:T(8,128)(2,1)}), bf16[32,1,16,2048]{3,2,1,0:T(8,128)(2,1)S(1)}, u32[]{:S(2)}, u32[]{:S(2)}) %all-to-all-start.1) | async-done | bytes 2097184 | tf_op jit(solution)/shard_map/all_to_all | solution.py:124
  80.5 7.4 %all-to-all-start.2 = ((bf16[16,1,32,1,2048]{4,2,3,1,0:T(8,128)(2,1)}), bf16[16,1,32,1,2048]{4,2,3,1,0:T(8,128)(2,1)S(1)}, u32[]{:S(2)}, u32[]{:S(2)}) async-start(bf16[16,1,32,1,2048]{4,2,3,1,0:T(8,128)(2,1)} %fusion.22), calls=%async_computation.2 | async-start | bytes 4194304 | tf_op jit(solution)/shard_map/all_to_all | solution.py:16
  89.9 44.6 %all-to-all-done.2 = bf16[16,1,32,1,2048]{4,2,3,1,0:T(8,128)(2,1)S(1)} async-done(((bf16[16,1,32,1,2048]{4,2,3,1,0:T(8,128)(2,1)}), bf16[16,1,32,1,2048]{4,2,3,1,0:T(8,128)(2,1)S(1)}, u32[]{:S(2)}, u32[]{:S(2)}) %all-to-all-start.2) | async-done | bytes 2097184 | tf_op jit(solution)/shard_map/all_to_all | solution.py:16
  134.5 10.4 %all-to-all-start = ((bf16[32,2,192]{2,1,0:T(2,128)(2,1)}), bf16[32,2,192]{2,1,0:T(2,128)(2,1)S(1)}, u32[]{:S(2)}, u32[]{:S(2)}) async-start(bf16[32,2,192]{2,1,0:T(2,128)(2,1)} %reshape.302), calls=%async_computation | async-start | bytes 65536 | tf_op jit(solution)/shard_map/all_to_all | solution.py:48
  150.7 7.8 %all-to-all-start.3 = ((bf16[32,2,1024]{2,1,0:T(2,128)(2,1)}), bf16[32,2,1024]{2,1,0:T(2,128)(2,1)S(1)}, u32[]{:S(2)}, u32[]{:S(2)}) async-start(bf16[32,2,1024]{2,1,0:T(2,128)(2,1)} %reshape.304), calls=%async_computation.3 | async-start | bytes 262144 | tf_op jit(solution)/shard_map/all_to_all | solution.py:135
  158.9 7.4 %all-to-all-done.3 = bf16[32,2,1024]{2,1,0:T(2,128)(2,1)S(1)} async-done(((bf16[32,2,1024]{2,1,0:T(2,128)(2,1)}), bf16[32,2,1024]{2,1,0:T(2,128)(2,1)S(1)}, u32[]{:S(2)}, u32[]{:S(2)}) %all-to-all-start.3) | async-done | bytes 131104 | tf_op jit(solution)/shard_map/all_to_all | solution.py:135
  168.1 7.4 %all-to-all-start.4 = ((bf16[16,1,32,1,2048]{4,2,3,1,0:T(8,128)(2,1)}), bf16[16,1,32,1,2048]{4,2,3,1,0:T(8,128)(2,1)}, u32[]{:S(2)}, u32[]{:S(2)}) async-start(bf16[16,1,32,1,2048]{4,2,3,1,0:T(8,128)(2,1)} %broadcast_in_dim.46), calls=%async_computation.4 | async-start | bytes 4194304 | tf_op jit(solution)/shard_map/all_to_all | solution.py:28
  175.5 10.9 %all-gather.5.cloned.1.call-done = bf16[12288,128]{1,0:T(8,128)(2,1)} async-done(((bf16[384,128]{1,0:T(8,128)(2,1)}), bf16[12288,128]{1,0:T(8,128)(2,1)}) %all-gather.5.cloned.1.call-update) | async-done | bytes 3145744 | tf_op jit(solution)/shard_map/all_gather | solution.py:45
  186.4 291.9 %while.13 = (s32[]{:T(128)}, bf16[32,1,384,128]{3,2,1,0:T(8,128)(2,1)}, f32[32,1,384]{2,1,0:T(1,128)S(1)}, s32[32]{0:T(128)S(1)}, s32[]{:T(128)}, /*index=5*/bf1...) while((s32[]{:T(128)}, ...), condition=%wide.region_6.7_spmd.clone, body=%wide.region_0.6_spmd.clone.sunk | while | flops 99241728 | bytes 5957639 | solution.py:90
  187.7 7.2 %conditional.3 = (bf16[1,1,384,128]{3,2,1,0:T(8,128)(2,1)S(1)}, f32[1,1,384]{2,1,0:T(1,128)S(1)}) conditional(s32[]{:T(128)} %convert_element_type.99, () %tuple.52, (s32[]{:T(128)}, s32[]{:T(128)}, bf16[32,384,1,128]{3,1,2,0:T(8,128)(2,1)}, s32[]{:T(128)}, bf16[384,1,128]{2,0,1:T(8,128)(2,1)S(1)}, /*index=5*/bf16[32,384,1]{1,0,2:T(8,128)(2,1)S(1)}, ...), branch_computations={%region_1.1_spmd, %region_2.5_spmd} | conditional | flops 99241728 | bytes 5755680 | solution.py:80
  251.6 7.2 %conditional.3 = (bf16[1,1,384,128]{3,2,1,0:T(8,128)(2,1)S(1)}, f32[1,1,384]{2,1,0:T(1,128)S(1)}) conditional(s32[]{:T(128)} %convert_element_type.99, () %tuple.52, (s32[]{:T(128)}, s32[]{:T(128)}, bf16[32,384,1,128]{3,1,2,0:T(8,128)(2,1)}, s32[]{:T(128)}, bf16[384,1,128]{2,0,1:T(8,128)(2,1)S(1)}, /*index=5*/bf16[32,384,1]{1,0,2:T(8,128)(2,1)S(1)}, ...), branch_computations={%region_1.1_spmd, %region_2.5_spmd} | conditional | flops 99241728 | bytes 5755680 | solution.py:80
  260.7 7.2 %conditional.3 = (bf16[1,1,384,128]{3,2,1,0:T(8,128)(2,1)S(1)}, f32[1,1,384]{2,1,0:T(1,128)S(1)}) conditional(s32[]{:T(128)} %convert_element_type.99, () %tuple.52, (s32[]{:T(128)}, s32[]{:T(128)}, bf16[32,384,1,128]{3,1,2,0:T(8,128)(2,1)}, s32[]{:T(128)}, bf16[384,1,128]{2,0,1:T(8,128)(2,1)S(1)}, /*index=5*/bf16[32,384,1]{1,0,2:T(8,128)(2,1)S(1)}, ...), branch_computations={%region_1.1_spmd, %region_2.5_spmd} | conditional | flops 99241728 | bytes 5755680 | solution.py:80
  269.8 7.2 %conditional.3 = (bf16[1,1,384,128]{3,2,1,0:T(8,128)(2,1)S(1)}, f32[1,1,384]{2,1,0:T(1,128)S(1)}) conditional(s32[]{:T(128)} %convert_element_type.99, () %tuple.52, (s32[]{:T(128)}, s32[]{:T(128)}, bf16[32,384,1,128]{3,1,2,0:T(8,128)(2,1)}, s32[]{:T(128)}, bf16[384,1,128]{2,0,1:T(8,128)(2,1)S(1)}, /*index=5*/bf16[32,384,1]{1,0,2:T(8,128)(2,1)S(1)}, ...), branch_computations={%region_1.1_spmd, %region_2.5_spmd} | conditional | flops 99241728 | bytes 5755680 | solution.py:80
  278.9 7.2 %conditional.3 = (bf16[1,1,384,128]{3,2,1,0:T(8,128)(2,1)S(1)}, f32[1,1,384]{2,1,0:T(1,128)S(1)}) conditional(s32[]{:T(128)} %convert_element_type.99, () %tuple.52, (s32[]{:T(128)}, s32[]{:T(128)}, bf16[32,384,1,128]{3,1,2,0:T(8,128)(2,1)}, s32[]{:T(128)}, bf16[384,1,128]{2,0,1:T(8,128)(2,1)S(1)}, /*index=5*/bf16[32,384,1]{1,0,2:T(8,128)(2,1)S(1)}, ...), branch_computations={%region_1.1_spmd, %region_2.5_spmd} | conditional | flops 99241728 | bytes 5755680 | solution.py:80
  288.0 7.2 %conditional.3 = (bf16[1,1,384,128]{3,2,1,0:T(8,128)(2,1)S(1)}, f32[1,1,384]{2,1,0:T(1,128)S(1)}) conditional(s32[]{:T(128)} %convert_element_type.99, () %tuple.52, (s32[]{:T(128)}, s32[]{:T(128)}, bf16[32,384,1,128]{3,1,2,0:T(8,128)(2,1)}, s32[]{:T(128)}, bf16[384,1,128]{2,0,1:T(8,128)(2,1)S(1)}, /*index=5*/bf16[32,384,1]{1,0,2:T(8,128)(2,1)S(1)}, ...), branch_computations={%region_1.1_spmd, %region_2.5_spmd} | conditional | flops 99241728 | bytes 5755680 | solution.py:80
  379.2 7.2 %conditional.3 = (bf16[1,1,384,128]{3,2,1,0:T(8,128)(2,1)S(1)}, f32[1,1,384]{2,1,0:T(1,128)S(1)}) conditional(s32[]{:T(128)} %convert_element_type.99, () %tuple.52, (s32[]{:T(128)}, s32[]{:T(128)}, bf16[32,384,1,128]{3,1,2,0:T(8,128)(2,1)}, s32[]{:T(128)}, bf16[384,1,128]{2,0,1:T(8,128)(2,1)S(1)}, /*index=5*/bf16[32,384,1]{1,0,2:T(8,128)(2,1)S(1)}, ...), branch_computations={%region_1.1_spmd, %region_2.5_spmd} | conditional | flops 99241728 | bytes 5755680 | solution.py:80
  388.4 7.2 %conditional.3 = (bf16[1,1,384,128]{3,2,1,0:T(8,128)(2,1)S(1)}, f32[1,1,384]{2,1,0:T(1,128)S(1)}) conditional(s32[]{:T(128)} %convert_element_type.99, () %tuple.52, (s32[]{:T(128)}, s32[]{:T(128)}, bf16[32,384,1,128]{3,1,2,0:T(8,128)(2,1)}, s32[]{:T(128)}, bf16[384,1,128]{2,0,1:T(8,128)(2,1)S(1)}, /*index=5*/bf16[32,384,1]{1,0,2:T(8,128)(2,1)S(1)}, ...), branch_computations={%region_1.1_spmd, %region_2.5_spmd} | conditional | flops 99241728 | bytes 5755680 | solution.py:80
  397.5 7.2 %conditional.3 = (bf16[1,1,384,128]{3,2,1,0:T(8,128)(2,1)S(1)}, f32[1,1,384]{2,1,0:T(1,128)S(1)}) conditional(s32[]{:T(128)} %convert_element_type.99, () %tuple.52, (s32[]{:T(128)}, s32[]{:T(128)}, bf16[32,384,1,128]{3,1,2,0:T(8,128)(2,1)}, s32[]{:T(128)}, bf16[384,1,128]{2,0,1:T(8,128)(2,1)S(1)}, /*index=5*/bf16[32,384,1]{1,0,2:T(8,128)(2,1)S(1)}, ...), branch_computations={%region_1.1_spmd, %region_2.5_spmd} | conditional | flops 99241728 | bytes 5755680 | solution.py:80
  415.7 7.2 %conditional.3 = (bf16[1,1,384,128]{3,2,1,0:T(8,128)(2,1)S(1)}, f32[1,1,384]{2,1,0:T(1,128)S(1)}) conditional(s32[]{:T(128)} %convert_element_type.99, () %tuple.52, (s32[]{:T(128)}, s32[]{:T(128)}, bf16[32,384,1,128]{3,1,2,0:T(8,128)(2,1)}, s32[]{:T(128)}, bf16[384,1,128]{2,0,1:T(8,128)(2,1)S(1)}, /*index=5*/bf16[32,384,1]{1,0,2:T(8,128)(2,1)S(1)}, ...), branch_computations={%region_1.1_spmd, %region_2.5_spmd} | conditional | flops 99241728 | bytes 5755680 | solution.py:80
  434.0 7.2 %conditional.3 = (bf16[1,1,384,128]{3,2,1,0:T(8,128)(2,1)S(1)}, f32[1,1,384]{2,1,0:T(1,128)S(1)}) conditional(s32[]{:T(128)} %convert_element_type.99, () %tuple.52, (s32[]{:T(128)}, s32[]{:T(128)}, bf16[32,384,1,128]{3,1,2,0:T(8,128)(2,1)}, s32[]{:T(128)}, bf16[384,1,128]{2,0,1:T(8,128)(2,1)S(1)}, /*index=5*/bf16[32,384,1]{1,0,2:T(8,128)(2,1)S(1)}, ...), branch_computations={%region_1.1_spmd, %region_2.5_spmd} | conditional | flops 99241728 | bytes 5755680 | solution.py:80
  443.1 7.2 %conditional.3 = (bf16[1,1,384,128]{3,2,1,0:T(8,128)(2,1)S(1)}, f32[1,1,384]{2,1,0:T(1,128)S(1)}) conditional(s32[]{:T(128)} %convert_element_type.99, () %tuple.52, (s32[]{:T(128)}, s32[]{:T(128)}, bf16[32,384,1,128]{3,1,2,0:T(8,128)(2,1)}, s32[]{:T(128)}, bf16[384,1,128]{2,0,1:T(8,128)(2,1)S(1)}, /*index=5*/bf16[32,384,1]{1,0,2:T(8,128)(2,1)S(1)}, ...), branch_computations={%region_1.1_spmd, %region_2.5_spmd} | conditional | flops 99241728 | bytes 5755680 | solution.py:80
  452.2 7.2 %conditional.3 = (bf16[1,1,384,128]{3,2,1,0:T(8,128)(2,1)S(1)}, f32[1,1,384]{2,1,0:T(1,128)S(1)}) conditional(s32[]{:T(128)} %convert_element_type.99, () %tuple.52, (s32[]{:T(128)}, s32[]{:T(128)}, bf16[32,384,1,128]{3,1,2,0:T(8,128)(2,1)}, s32[]{:T(128)}, bf16[384,1,128]{2,0,1:T(8,128)(2,1)S(1)}, /*index=5*/bf16[32,384,1]{1,0,2:T(8,128)(2,1)S(1)}, ...), branch_computations={%region_1.1_spmd, %region_2.5_spmd} | conditional | flops 99241728 | bytes 5755680 | solution.py:80
  461.4 7.2 %conditional.3 = (bf16[1,1,384,128]{3,2,1,0:T(8,128)(2,1)S(1)}, f32[1,1,384]{2,1,0:T(1,128)S(1)}) conditional(s32[]{:T(128)} %convert_element_type.99, () %tuple.52, (s32[]{:T(128)}, s32[]{:T(128)}, bf16[32,384,1,128]{3,1,2,0:T(8,128)(2,1)}, s32[]{:T(128)}, bf16[384,1,128]{2,0,1:T(8,128)(2,1)S(1)}, /*index=5*/bf16[32,384,1]{1,0,2:T(8,128)(2,1)S(1)}, ...), branch_computations={%region_1.1_spmd, %region_2.5_spmd} | conditional | flops 99241728 | bytes 5755680 | solution.py:80
  470.5 7.2 %conditional.3 = (bf16[1,1,384,128]{3,2,1,0:T(8,128)(2,1)S(1)}, f32[1,1,384]{2,1,0:T(1,128)S(1)}) conditional(s32[]{:T(128)} %convert_element_type.99, () %tuple.52, (s32[]{:T(128)}, s32[]{:T(128)}, bf16[32,384,1,128]{3,1,2,0:T(8,128)(2,1)}, s32[]{:T(128)}, bf16[384,1,128]{2,0,1:T(8,128)(2,1)S(1)}, /*index=5*/bf16[32,384,1]{1,0,2:T(8,128)(2,1)S(1)}, ...), branch_computations={%region_1.1_spmd, %region_2.5_spmd} | conditional | flops 99241728 | bytes 5755680 | solution.py:80
  (563 shorter events, 440.3 us)
Async XLA Ops:
  7.2 71.2 %copy-start = (bf16[1,224,2048]{2,1,0:T(8,128)(2,1)S(1)}, bf16[1,224,2048]{2,1,0:T(8,128)(2,1)}, u32[]{:S(2)}) copy-start(bf16[1,224,2048]{2,1,0:T(8,128)(2,1)} %param.23) | copy-start | bytes 2752516
  7.2 168.3 %all-gather.3.cloned.1.call-start = ((), (), s32[]{:S(2)}) async-start(), calls=%async_computation.5 | async-start | bytes 3244032 | tf_op jit(solution)/shard_map/all_gather | solution.py:44
  17.3 58.4 %all-to-all-start.1 = ((bf16[32,1,16,2048]{3,2,1,0:T(8,128)(2,1)}), bf16[32,1,16,2048]{3,2,1,0:T(8,128)(2,1)S(1)}, u32[]{:S(2)}, u32[]{:S(2)}) async-start(bf16[32,1,16,2048]{3,2,1,0:T(8,128)(2,1)} %bitcast.23), calls=%async_computation.1 | async-start | bytes 4194304 | tf_op jit(solution)/shard_map/all_to_all | solution.py:124
  24.4 162.0 %all-gather.5.cloned.1.call-start = ((), (), s32[]{:S(2)}) async-start(), calls=%async_computation.6 | async-start | bytes 3244032 | tf_op jit(solution)/shard_map/all_gather | solution.py:45
  75.6 2.0 copy-start.3
  80.5 7.4 %copy-start.1 = (bf16[384,1]{0,1:T(2,128)(2,1)S(1)}, bf16[384,1]{0,1:T(2,128)(2,1)}, u32[]{:S(2)}) copy-start(bf16[384,1]{0,1:T(2,128)(2,1)} %param.18) | copy-start | bytes 2308
  80.5 54.0 %all-to-all-start.2 = ((bf16[16,1,32,1,2048]{4,2,3,1,0:T(8,128)(2,1)}), bf16[16,1,32,1,2048]{4,2,3,1,0:T(8,128)(2,1)S(1)}, u32[]{:S(2)}, u32[]{:S(2)}) async-start(bf16[16,1,32,1,2048]{4,2,3,1,0:T(8,128)(2,1)} %fusion.22), calls=%async_computation.2 | async-start | bytes 4194304 | tf_op jit(solution)/shard_map/all_to_all | solution.py:16
  87.8 70.8 %copy-start.2 = (f32[128,2]{0,1:T(2,128)S(1)}, f32[128,2]{0,1:T(2,128)}, u32[]{:S(2)}) copy-start(f32[128,2]{0,1:T(2,128)} %param.25) | copy-start | bytes 3076
  134.5 16.2 %all-to-all-start = ((bf16[32,2,192]{2,1,0:T(2,128)(2,1)}), bf16[32,2,192]{2,1,0:T(2,128)(2,1)S(1)}, u32[]{:S(2)}, u32[]{:S(2)}) async-start(bf16[32,2,192]{2,1,0:T(2,128)(2,1)} %reshape.302), calls=%async_computation | async-start | bytes 65536 | tf_op jit(solution)/shard_map/all_to_all | solution.py:48
  150.7 15.5 %all-to-all-start.3 = ((bf16[32,2,1024]{2,1,0:T(2,128)(2,1)}), bf16[32,2,1024]{2,1,0:T(2,128)(2,1)S(1)}, u32[]{:S(2)}, u32[]{:S(2)}) async-start(bf16[32,2,1024]{2,1,0:T(2,128)(2,1)} %reshape.304), calls=%async_computation.3 | async-start | bytes 262144 | tf_op jit(solution)/shard_map/all_to_all | solution.py:135
  168.1 18.3 %copy-start.4 = (bf16[384,128]{1,0:T(8,128)(2,1)S(1)}, bf16[384,128]{1,0:T(8,128)(2,1)}, u32[]{:S(2)}) copy-start(bf16[384,128]{1,0:T(8,128)(2,1)} %param.15) | copy-start | bytes 294916
  168.1 315.1 %all-to-all-start.4 = ((bf16[16,1,32,1,2048]{4,2,3,1,0:T(8,128)(2,1)}), bf16[16,1,32,1,2048]{4,2,3,1,0:T(8,128)(2,1)}, u32[]{:S(2)}, u32[]{:S(2)}) async-start(bf16[16,1,32,1,2048]{4,2,3,1,0:T(8,128)(2,1)} %broadcast_in_dim.46), calls=%async_computation.4 | async-start | bytes 4194304 | tf_op jit(solution)/shard_map/all_to_all | solution.py:28
Sparse Core Ops, SparseCore 0:
  11.1 88.8 all-gather.2
  103.2 83.1 all-gather.4
